TPU v7x, 32 devices: a whole 2x2x4 slice. The times are simulated.
32 devices in a mesh: sp: 4 (over z), dp: 8 (over y, x, core).
Axes of the slice: x: 2, y: 2, z: 4, core: 2. Of those that a mesh axis runs over, the one named last changes fastest.
Arguments:
- up_pre: bfloat16 [8, 1536, 2048], P('dp', 'sp'), may hold values from -6 to 6
- mix_pre: bfloat16 [8, 1536, 2048], P('dp', 'sp'), may hold values from -6 to 6
- ln_gain: float32 [2048], replicated, may hold values from 0.1 to 1.9
- mix_weight: bfloat16 [16, 128, 128], replicated, may hold values from -0.5 to 0.5
- mix_bias: float32 [16, 128], replicated, may hold values from 0.1 to 1.9
- out_weight: bfloat16 [2048, 2048], P('sp', 'dp'), may hold values from -0.125 to 0.125
Outputs:
- mixed_out: bfloat16 [8, 1536, 2048], P('dp', 'sp')
All inputs are finite; a program needn't handle non-finite values.
Results may differ from a plain program's by a relative error of at most 0.012.
Values may be sent and summed in bfloat16 or wider, within the bound.
A program may use at most 64 MiB of HBM per device.

v0:
```python
import jax
import jax.numpy as jnp
from jax import lax
from jax.sharding import PartitionSpec as P

BLOCK = 128
norm_epsilon = 1e-05


def normalize(up_rows, mix_rows, ln_gain):
    up_act = jax.nn.gelu(up_rows.astype(jnp.float32), approximate=False).astype(jnp.bfloat16)
    activated = jax.nn.gelu(mix_rows.astype(jnp.float32), approximate=False)
    center = jnp.mean(activated, axis=-1, keepdims=True)
    spread = jnp.mean(jnp.square(activated - center), axis=-1, keepdims=True)
    normed = ((activated - center) * lax.rsqrt(spread + norm_epsilon) * ln_gain).astype(
        jnp.bfloat16
    )
    return (up_act, normed)


def mix_blocks(up_act, normed, local_weight, local_bias):
    row_count, channels = normed.shape
    local_groups = local_weight.shape[0]
    blocks = normed.reshape(row_count // BLOCK, BLOCK, local_groups, channels // local_groups)
    mixed_sum = jnp.einsum(
        "gts,nsgc->ntgc", local_weight, blocks, preferred_element_type=jnp.float32
    )
    mixed_sum = mixed_sum + jnp.transpose(local_bias)[None, :, :, None]
    return (up_act.astype(jnp.float32) * mixed_sum.reshape(row_count, channels)).astype(
        jnp.bfloat16
    )


def per_device(up_pre, mix_pre, ln_gain, mix_weight, mix_bias, out_weight):
    up_act, normed = normalize(up_pre[0], mix_pre[0], ln_gain)
    positions = lax.broadcasted_iota(jnp.int32, (BLOCK, BLOCK), 0)
    sources = lax.broadcasted_iota(jnp.int32, (BLOCK, BLOCK), 1)
    causal = positions >= sources
    masked = jnp.where(causal[None], mix_weight, jnp.zeros_like(mix_weight))
    gated = mix_blocks(up_act, normed, masked, mix_bias)
    rows_whole = lax.all_gather(out_weight, "sp", axis=0, tiled=True)
    result = jnp.dot(
        gated,
        lax.all_gather(rows_whole, "dp", axis=1, tiled=True),
        preferred_element_type=jnp.float32,
    )
    return result.astype(jnp.bfloat16)[None]


def solution(mesh):
    return jax.shard_map(
        per_device,
        mesh=mesh,
        in_specs=(P("dp", "sp", None), P("dp", "sp", None), P(), P(), P(), P("sp", "dp")),
        out_specs=P("dp", "sp", None),
        check_vma=False,
    )
```

profile of v0, /device:TPU:0, one launch (start us, length us, event | category | flops | bytes accessed | tf_op | source)
XLA Modules:
  0.0 118.3 jit_solution(18165163851771315332)
XLA Ops:
  6.5 0.0 all-gather.3.cloned.1.call-start
  6.5 0.7 all-gather.3.cloned.1.call-update
  7.3 0.0 all-gather.5.cloned.1.call-start
  7.3 32.3 %all-gather.3.cloned.1.call-done = bf16[2048,256]{1,0:T(8,128)(2,1)} async-done(((bf16[512,256]{1,0:T(8,128)(2,1)}), bf16[2048,256]{1,0:T(8,128)(2,1)}) %all-gather.3.cloned.1.call-update) | async-done | bytes 1048592 | tf_op jit(solution)/shard_map/all_gather | solution.py:41
  39.6 0.0 all-gather.5.cloned.1.call-update
  39.7 3.6 %fusion.38 = (f32[48,8,16,128]{3,1,2,0:T(8,128)S(1)}, f32[48,8,16,128]{3,1,2,0:T(8,128)}) fusion(bf16[1,384,2048]{2,1,0:T(8,128)(2,1)} %param.7), kind=kLoop, calls=%fused_computation.45 | loop fusion | flops 3145728 | bytes 7864320
  43.2 0.7 copy.22
  43.9 2.4 %copy.13 = f32[3,128,16,128]{1,3,0,2:T(8,128)} copy(f32[3,128,16,128]{3,2,1,0:T(8,128)S(1)} %bitcast.227) | data formatting | bytes 6291456 | tf_op jit(solution)/shard_map/mul | solution.py:12
  46.3 2.9 %copy.21 = f32[48,8,16,128]{3,2,1,0:T(8,128)S(1)} copy(f32[48,8,16,128]{3,1,2,0:T(8,128)} %get-tuple-element.8) | data formatting | bytes 6291456
  49.2 2.4 %copy.18 = f32[3,128,16,128]{1,3,0,2:T(8,128)} copy(f32[3,128,16,128]{3,2,1,0:T(8,128)S(1)} %bitcast.228) | data formatting | bytes 6291456 | tf_op jit(solution)/shard_map/mul | solution.py:12
  51.7 0.0 copy-start
  51.7 0.0 copy-start.1
  51.7 0.0 copy-start.2
  51.7 0.0 copy-start.3
  51.7 0.0 copy-start.4
  51.7 8.6 %fusion.177 = (f32[384]{0:T(512)S(1)}, f32[384,2048]{1,0:T(8,128)S(1)}) fusion(bf16[1,384,2048]{2,1,0:T(8,128)(2,1)} %param.7), kind=kLoop, calls=%fused_computation.196 | loop fusion | flops 51904128 | bytes 4720128 | tf_op jit(solution)/shard_map/reduce_sum | solution.py:13
  60.4 0.5 multiply_reduce_fusion
  60.9 0.0 copy-done
  60.9 0.0 copy-done.1
  60.9 0.0 copy-done.2
  60.9 0.0 copy-done.3
  60.9 0.0 copy-done.4
  60.9 8.6 %bitcast_add_fusion = f32[3,128,16,128]{1,3,0,2:T(8,128)} fusion(f32[128,16]{0,1:T(8,128)S(1)} %bitcast.230, f32[3,128,16,128]{1,3,0,2:T(8,128)S(1)} %copy-done.1, f32[3,128,16,128]{1,3,0,2:T(8,128)S(1)} %copy-done, f32[16,128]{1,0:T(8,128)S(1)} %bitcast.231, f32[3,128]{1,0:T(4,128)S(1)} %rsqrt_bitcast_fusion, f32[3,128]{1,0:T(4,128)S(1)} %get-tuple-element.9, ...), kind=kOutput, calls=%fused_computation.82 | convolution fusion | flops 253493248 | bytes 9997312 | tf_op jit(solution)/shard_map/gts,nsgc->ntgc/dot_general | solution.py:25
  69.5 2.7 %copy.19 = f32[3,128,16,128]{3,2,1,0:T(8,128)S(1)} copy(f32[3,128,16,128]{1,3,0,2:T(8,128)} %bitcast_add_fusion) | data formatting | bytes 6291456 | tf_op jit(solution)/shard_map/add | solution.py:28
  72.2 24.6 %all-gather.5.cloned.1.call-done = bf16[2048,2048]{1,0:T(8,128)(2,1)} async-done(((bf16[2048,256]{1,0:T(8,128)(2,1)}), bf16[2048,2048]{1,0:T(8,128)(2,1)}) %all-gather.5.cloned.1.call-update) | async-done | bytes 8388624 | tf_op jit(solution)/shard_map/all_gather | solution.py:44
  96.8 14.7 %fusion.80 = bf16[1,384,2048]{2,1,0:T(8,128)(2,1)} fusion(bf16[2048,2048]{1,0:T(8,128)(2,1)} %all-gather.5.cloned.1.call-done, f32[48,8,16,128]{3,2,1,0:T(8,128)S(1)} %bitcast.229, bf16[1,384,2048]{2,1,0:T(8,128)(2,1)} %param.6), kind=kOutput, calls=%fused_computation.98 | convolution fusion | flops 3276275712 | bytes 14680064 | tf_op jit(solution)/shard_map/dot_general | solution.py:42
  (3 shorter events, 0.0 us)
Async XLA Ops:
  6.5 33.1 %all-gather.3.cloned.1.call-start = ((), (), s32[]{:S(2)}) async-start(), calls=%async_computation | async-start | bytes 1310720 | tf_op jit(solution)/shard_map/all_gather | solution.py:41
  7.3 89.5 %all-gather.5.cloned.1.call-start = ((), (), s32[]{:S(2)}) async-start(), calls=%async_computation.1 | async-start | bytes 9437184 | tf_op jit(solution)/shard_map/all_gather | solution.py:44
  51.7 9.2 %copy-start = (f32[3,128,16,128]{1,3,0,2:T(8,128)S(1)}, f32[3,128,16,128]{1,3,0,2:T(8,128)}, u32[]{:S(2)}) copy-start(f32[3,128,16,128]{1,3,0,2:T(8,128)} %copy.13) | copy-start | bytes 9437188
  51.7 9.2 %copy-start.1 = (f32[3,128,16,128]{1,3,0,2:T(8,128)S(1)}, f32[3,128,16,128]{1,3,0,2:T(8,128)}, u32[]{:S(2)}) copy-start(f32[3,128,16,128]{1,3,0,2:T(8,128)} %copy.18) | copy-start | bytes 9437188
  51.7 9.2 %copy-start.2 = (bf16[16,128,128]{2,1,0:T(8,128)(2,1)S(1)}, bf16[16,128,128]{2,1,0:T(8,128)(2,1)}, u32[]{:S(2)}) copy-start(bf16[16,128,128]{2,1,0:T(8,128)(2,1)} %param.9) | copy-start | bytes 1572868
  51.7 9.2 %copy-start.3 = (f32[16,128]{1,0:T(8,128)S(1)}, f32[16,128]{1,0:T(8,128)}, u32[]{:S(2)}) copy-start(f32[16,128]{1,0:T(8,128)} %param.10) | copy-start | bytes 24580
  51.7 9.2 %copy-start.4 = (f32[2048]{0:T(1024)S(1)}, f32[2048]{0:T(1024)}, u32[]{:S(2)}) copy-start(f32[2048]{0:T(1024)} %param.8) | copy-start | bytes 24580
Sparse Core Ops, SparseCore 0:
  8.9 30.6 all-gather.2
  41.5 55.2 all-gather.4
where the time goes:
time: 118 us
  waiting for transfers between devices  57.7 us (49%)
  matrix products  23.3 us (20%)
  between operations  13.5 us (11%)
  other arithmetic  12.7 us (11%)
  local copies, waits for them, and re-layouts  11.1 us (9%)
    all_gather x1, waiting for transfers between devices, per_device(): rows_whole = lax.all_gather(out_weight, 'sp', axis=0, tiled=True)  32.3 us
    all_gather x1, waiting for transfers between devices, per_device(): lax.all_gather(rows_whole, 'dp', axis=1, tiled=True)  24.6 us
    dot_general x1, matrix products, per_device(): jnp.dot(gated, lax.all_gather(rows_whole, 'dp', axis=1, tiled=True), pref...  14.7 us
    reduce_sum x1, other arithmetic, normalize(): center = jnp.mean(activated, axis=-1, keepdims=True)  8.65 us
    dot_general x1, matrix products, mix_blocks(): jnp.einsum('gts,nsgc->ntgc', local_weight, blocks, preferred_element_type...  8.6 us
    mul x2, local copies, waits for them, and re-layouts, normalize(): activated = jax.nn.gelu(mix_rows.astype(jnp.float32), approximate=False)  4.86 us
    unnamed x1, other arithmetic  3.58 us
    unnamed x12, local copies, waits for them, and re-layouts  3.57 us
  transfers between devices with their start and end apart: 2, of which 2 were waited for; matrix products, arithmetic and copies ran while one was open for 27% of the time, Pallas kernels for 0%

commit v1 on v0

--- a/solution.py
+++ b/solution.py
@@ -38,7 +38,12 @@
     causal = positions >= sources
     masked = jnp.where(causal[None], mix_weight, jnp.zeros_like(mix_weight))
     gated = mix_blocks(up_act, normed, masked, mix_bias)
-    rows_whole = lax.all_gather(out_weight, "sp", axis=0, tiled=True)
+    ring = [out_weight]
+    for hop in range(3):
+        ring.append(lax.ppermute(ring[-1], "sp", [(dev, (dev + 1) % 4) for dev in range(4)]))
+    rows_whole = jnp.roll(
+        jnp.concatenate(ring[::-1], axis=0), (lax.axis_index("sp") + 1) * ring[0].shape[0], axis=0
+    )
     result = jnp.dot(
         gated,
         lax.all_gather(rows_whole, "dp", axis=1, tiled=True),

time: 118 us -> 114 us (0.966)
  waiting for transfers between devices: 57.7 us -> 49.2 us
  starting transfers between devices: 0.04 us -> 3.06 us
  local copies, waits for them, and re-layouts: 11.1 us -> 13.2 us
  other arithmetic: 12.7 us -> 11.3 us
    all_gather x1 -> x0, waiting for transfers between devices: 32.3 us -> none  [per_device(): rows_whole = lax.all_gather(out_weight, 'sp', axis=0, tiled=True)]
    ppermute x0 -> x3, waiting for transfers between devices: none -> 26.3 us  [per_device(): lax.ppermute(ring[-1], 'sp', [(dev, (dev + 1) % 4) for dev in range(4)])]
    ppermute x0 -> x3, starting transfers between devices: none -> 3.06 us  [per_device(): lax.ppermute(ring[-1], 'sp', [(dev, (dev + 1) % 4) for dev in range(4)])]
    all_gather x1, waiting for transfers between devices: 24.6 us -> 22.9 us  [per_device(): lax.all_gather(rows_whole, 'dp', axis=1, tiled=True)]
    unnamed x1, other arithmetic: 3.58 us -> 2.19 us
    unnamed x12 -> x23, local copies, waits for them, and re-layouts: 3.57 us -> 4.67 us
  transfers between devices with their start and end apart: 2 -> 4, of which waited for: 2 -> 4; matrix products, arithmetic and copies ran while one was open for 27% -> 27% of each run, Pallas kernels for 0% -> 0%
where the time goes in v1:
time: 114 us
  waiting for transfers between devices  49.2 us (43%)
  matrix products  23.3 us (20%)
  between operations  13.6 us (12%)
  local copies, waits for them, and re-layouts  13.2 us (12%)
  other arithmetic  11.3 us (10%)
  starting transfers between devices  3.06 us (3%)
    ppermute x3, waiting for transfers between devices, per_device(): lax.ppermute(ring[-1], 'sp', [(dev, (dev + 1) % 4) for dev in range(4)])  26.3 us
    all_gather x1, waiting for transfers between devices, per_device(): lax.all_gather(rows_whole, 'dp', axis=1, tiled=True)  22.9 us
    dot_general x1, matrix products, per_device(): jnp.dot(gated, lax.all_gather(rows_whole, 'dp', axis=1, tiled=True), pref...  14.7 us
    reduce_sum x1, other arithmetic, normalize(): center = jnp.mean(activated, axis=-1, keepdims=True)  8.64 us
    dot_general x1, matrix products, mix_blocks(): jnp.einsum('gts,nsgc->ntgc', local_weight, blocks, preferred_element_type...  8.6 us
    mul x2, local copies, waits for them, and re-layouts, normalize(): activated = jax.nn.gelu(mix_rows.astype(jnp.float32), approximate=False)  4.86 us
    unnamed x23, local copies, waits for them, and re-layouts  4.67 us
    ppermute x3, starting transfers between devices, per_device(): lax.ppermute(ring[-1], 'sp', [(dev, (dev + 1) % 4) for dev in range(4)])  3.06 us
  transfers between devices with their start and end apart: 4, of which 4 were waited for; matrix products, arithmetic and copies ran while one was open for 27% of the time, Pallas kernels for 0%

profile of v1, /device:TPU:0, one launch (start us, length us, event | category | flops | bytes accessed | tf_op | source)
XLA Modules:
  0.0 113.7 jit_solution(14521850731216499361)
XLA Ops:
  6.5 0.0 copy-start.3
  6.5 0.0 all-gather.2.cloned.1.call-start
  6.5 3.1 %collective-permute-start = (bf16[512,256]{1,0:T(8,128)(2,1)}, bf16[512,256]{1,0:T(8,128)(2,1)S(1)}, u32[]{:S(2)}, u32[]{:S(2)}) collective-permute-start(bf16[512,256]{1,0:T(8,128)(2,1)} %param.11), channel_id=1, source_target_pairs={{0,8},{8,16},{16,24},{24,0},{1,9},{9,17},{17,25},{25,1},{2,10},{10... | collective-permute-start | bytes 786440 | tf_op jit(solution)/shard_map/ppermute | solution.py:43
  9.6 8.6 %collective-permute-done = bf16[512,256]{1,0:T(8,128)(2,1)S(1)} collective-permute-done((bf16[512,256]{1,0:T(8,128)(2,1)}, bf16[512,256]{1,0:T(8,128)(2,1)S(1)}, u32[]{:S(2)}, u32[]{:S(2)}) %collective-permute-start) | collective-permute-done | bytes 262176 | tf_op jit(solution)/shard_map/ppermute | solution.py:43
  18.2 0.0 collective-permute-start.1
  18.2 9.3 %collective-permute-done.1 = bf16[512,256]{1,0:T(8,128)(2,1)S(1)} collective-permute-done((bf16[512,256]{1,0:T(8,128)(2,1)S(1)}, bf16[512,256]{1,0:T(8,128)(2,1)S(1)}, u32[]{:S(2)}, u32[]{:S(2)}) %collective-permute-start.1) | collective-permute-done | bytes 262176 | tf_op jit(solution)/shard_map/ppermute | solution.py:43
  27.5 0.0 collective-permute-start.2
  27.5 8.4 %collective-permute-done.2 = bf16[512,256]{1,0:T(8,128)(2,1)S(1)} collective-permute-done((bf16[512,256]{1,0:T(8,128)(2,1)S(1)}, bf16[512,256]{1,0:T(8,128)(2,1)S(1)}, u32[]{:S(2)}, u32[]{:S(2)}) %collective-permute-start.2) | collective-permute-done | bytes 262176 | tf_op jit(solution)/shard_map/ppermute | solution.py:43
  35.9 0.0 copy-start
  36.0 1.1 constant_dynamic-update-slice_fusion.4
  37.1 0.0 copy-done.3
  37.2 1.0 constant_dynamic-slice_fusion
  38.2 0.0 all-gather.2.cloned.1.call-update
  38.2 0.0 copy-done
  38.3 2.2 %fusion.38 = (f32[48,8,16,128]{3,1,2,0:T(8,128)S(1)}, f32[48,8,16,128]{3,1,2,0:T(8,128)}) fusion(bf16[1,384,2048]{2,1,0:T(8,128)(2,1)S(1)} %copy-done), kind=kLoop, calls=%fused_computation.45 | loop fusion | flops 3145728 | bytes 7864320
  40.4 0.7 copy.22
  41.1 2.4 %copy.13 = f32[3,128,16,128]{1,3,0,2:T(8,128)} copy(f32[3,128,16,128]{3,2,1,0:T(8,128)S(1)} %bitcast.227) | data formatting | bytes 6291456 | tf_op jit(solution)/shard_map/mul | solution.py:12
  43.5 2.8 %copy.21 = f32[48,8,16,128]{3,2,1,0:T(8,128)S(1)} copy(f32[48,8,16,128]{3,1,2,0:T(8,128)} %get-tuple-element.8) | data formatting | bytes 6291456
  46.3 2.4 %copy.18 = f32[3,128,16,128]{1,3,0,2:T(8,128)} copy(f32[3,128,16,128]{3,2,1,0:T(8,128)S(1)} %bitcast.228) | data formatting | bytes 6291456 | tf_op jit(solution)/shard_map/mul | solution.py:12
  48.8 0.0 copy-start.1
  48.8 0.0 copy-start.2
  48.8 0.0 copy-start.4
  48.8 0.0 copy-start.5
  48.8 0.0 copy-start.6
  48.8 8.6 %fusion.177 = (f32[384]{0:T(512)S(1)}, f32[384,2048]{1,0:T(8,128)S(1)}) fusion(bf16[1,384,2048]{2,1,0:T(8,128)(2,1)} %param.7), kind=kLoop, calls=%fused_computation.205 | loop fusion | flops 51904128 | bytes 4720128 | tf_op jit(solution)/shard_map/reduce_sum | solution.py:13
  57.5 0.5 multiply_reduce_fusion
  57.9 0.0 copy-done.1
  58.0 0.0 copy-done.2
  58.0 0.0 copy-done.4
  58.0 0.0 copy-done.5
  58.0 0.0 copy-done.6
  58.0 8.6 %bitcast_add_fusion = f32[3,128,16,128]{1,3,0,2:T(8,128)} fusion(f32[128,16]{0,1:T(8,128)S(1)} %bitcast.230, f32[3,128,16,128]{1,3,0,2:T(8,128)S(1)} %copy-done.2, f32[3,128,16,128]{1,3,0,2:T(8,128)S(1)} %copy-done.1, f32[16,128]{1,0:T(8,128)S(1)} %bitcast.231, f32[3,128]{1,0:T(4,128)S(1)} %rsqrt_bitcast_fusion, f32[3,128]{1,0:T(4,128)S(1)} %get-tuple-element.9, ...), kind=kOutput, calls=%fused_computation.82 | convolution fusion | flops 253493248 | bytes 9997312 | tf_op jit(solution)/shard_map/gts,nsgc->ntgc/dot_general | solution.py:25
  66.6 2.7 %copy.19 = f32[3,128,16,128]{3,2,1,0:T(8,128)S(1)} copy(f32[3,128,16,128]{1,3,0,2:T(8,128)} %bitcast_add_fusion) | data formatting | bytes 6291456 | tf_op jit(solution)/shard_map/add | solution.py:28
  69.3 22.9 %all-gather.2.cloned.1.call-done = bf16[2048,2048]{1,0:T(8,128)(2,1)} async-done(((bf16[2048,256]{1,0:T(8,128)(2,1)}), bf16[2048,2048]{1,0:T(8,128)(2,1)}) %all-gather.2.cloned.1.call-update) | async-done | bytes 8388624 | tf_op jit(solution)/shard_map/all_gather | solution.py:49
  92.2 14.7 %fusion.80 = bf16[1,384,2048]{2,1,0:T(8,128)(2,1)} fusion(bf16[2048,2048]{1,0:T(8,128)(2,1)} %all-gather.2.cloned.1.call-done, f32[48,8,16,128]{3,2,1,0:T(8,128)S(1)} %bitcast.229, bf16[1,384,2048]{2,1,0:T(8,128)(2,1)} %param.6), kind=kOutput, calls=%fused_computation.98 | convolution fusion | flops 3276275712 | bytes 14680064 | tf_op jit(solution)/shard_map/dot_general | solution.py:47
  (10 shorter events, 0.2 us)
Async XLA Ops:
  6.5 30.6 %copy-start.3 = (bf16[512,256]{1,0:T(8,128)(2,1)S(1)}, bf16[512,256]{1,0:T(8,128)(2,1)}, u32[]{:S(2)}) copy-start(bf16[512,256]{1,0:T(8,128)(2,1)} %param.11) | copy-start | bytes 786436
  6.5 85.6 %all-gather.2.cloned.1.call-start = ((), (), s32[]{:S(2)}) async-start(), calls=%async_computation | async-start | bytes 9437184 | tf_op jit(solution)/shard_map/all_gather | solution.py:49
  6.5 11.7 %collective-permute-start = (bf16[512,256]{1,0:T(8,128)(2,1)}, bf16[512,256]{1,0:T(8,128)(2,1)S(1)}, u32[]{:S(2)}, u32[]{:S(2)}) collective-permute-start(bf16[512,256]{1,0:T(8,128)(2,1)} %param.11), channel_id=1, source_target_pairs={{0,8},{8,16},{16,24},{24,0},{1,9},{9,17},{17,25},{25,1},{2,10},{10... | collective-permute-start | bytes 786440 | tf_op jit(solution)/shard_map/ppermute | solution.py:43
  18.2 9.3 %collective-permute-start.1 = (bf16[512,256]{1,0:T(8,128)(2,1)S(1)}, bf16[512,256]{1,0:T(8,128)(2,1)S(1)}, u32[]{:S(2)}, u32[]{:S(2)}) collective-permute-start(bf16[512,256]{1,0:T(8,128)(2,1)S(1)} %collective-permute-done), channel_id=1, source_target_pairs={{0,8},{8,16},{16,24},{24,0},{1,9},{9,17},{17,25},{25,1},{2,10},{10... | collective-permute-start | bytes 786440 | tf_op jit(solution)/shard_map/ppermute | solution.py:43
  27.5 8.4 %collective-permute-start.2 = (bf16[512,256]{1,0:T(8,128)(2,1)S(1)}, bf16[512,256]{1,0:T(8,128)(2,1)S(1)}, u32[]{:S(2)}, u32[]{:S(2)}) collective-permute-start(bf16[512,256]{1,0:T(8,128)(2,1)S(1)} %collective-permute-done.1), channel_id=1, source_target_pairs={{0,8},{8,16},{16,24},{24,0},{1,9},{9,17},{17,25},{25,1},{2,10},{10... | collective-permute-start | bytes 786440 | tf_op jit(solution)/shard_map/ppermute | solution.py:43
  35.9 2.3 %copy-start = (bf16[1,384,2048]{2,1,0:T(8,128)(2,1)S(1)}, bf16[1,384,2048]{2,1,0:T(8,128)(2,1)}, u32[]{:S(2)}) copy-start(bf16[1,384,2048]{2,1,0:T(8,128)(2,1)} %param.7) | copy-start | bytes 4718596
  48.8 9.2 %copy-start.1 = (f32[3,128,16,128]{1,3,0,2:T(8,128)S(1)}, f32[3,128,16,128]{1,3,0,2:T(8,128)}, u32[]{:S(2)}) copy-start(f32[3,128,16,128]{1,3,0,2:T(8,128)} %copy.13) | copy-start | bytes 9437188
  48.8 9.2 %copy-start.2 = (f32[3,128,16,128]{1,3,0,2:T(8,128)S(1)}, f32[3,128,16,128]{1,3,0,2:T(8,128)}, u32[]{:S(2)}) copy-start(f32[3,128,16,128]{1,3,0,2:T(8,128)} %copy.18) | copy-start | bytes 9437188
  48.8 9.2 %copy-start.4 = (bf16[16,128,128]{2,1,0:T(8,128)(2,1)S(1)}, bf16[16,128,128]{2,1,0:T(8,128)(2,1)}, u32[]{:S(2)}) copy-start(bf16[16,128,128]{2,1,0:T(8,128)(2,1)} %param.9) | copy-start | bytes 1572868
  48.8 9.2 %copy-start.5 = (f32[16,128]{1,0:T(8,128)S(1)}, f32[16,128]{1,0:T(8,128)}, u32[]{:S(2)}) copy-start(f32[16,128]{1,0:T(8,128)} %param.10) | copy-start | bytes 24580
  48.8 9.2 %copy-start.6 = (f32[2048]{0:T(1024)S(1)}, f32[2048]{0:T(1024)}, u32[]{:S(2)}) copy-start(f32[2048]{0:T(1024)} %param.8) | copy-start | bytes 24580
Sparse Core Ops, SparseCore 0:
  38.4 53.7 all-gather.1
